TPU v7x, 32 devices: a whole 2x2x4 slice. The times are simulated.
32 devices in a mesh: sp: 16 (over z, y, x), tp: 2 (over core).
Axes of the slice: x: 2, y: 2, z: 4, core: 2. Of those that a mesh axis runs over, the one named last changes fastest.
Arguments:
- stream: bfloat16 [2048, 2048], P('sp'), may hold values from -6 to 6
- query_narrow: bfloat16 [2048, 512], P('sp', 'tp'), may hold values from -7 to 7
- query_broad: bfloat16 [2048, 1024], P('sp', 'tp'), may hold values from -7 to 7
- key_narrow: bfloat16 [2048, 512], P('sp', 'tp'), may hold values from -7 to 7
- key_broad: bfloat16 [2048, 1024], P('sp', 'tp'), may hold values from -7 to 7
- value_narrow: bfloat16 [2048, 512], P('sp', 'tp'), may hold values from -6 to 6
- value_broad: bfloat16 [2048, 1024], P('sp', 'tp'), may hold values from -6 to 6
- key_offsets: float32 [2048, 16], P('sp', 'tp'), may hold values from -20 to 0
- out_narrow: bfloat16 [512, 2048], P('tp'), may hold values from -0.4375 to 0.4375
- out_broad: bfloat16 [1024, 2048], P('tp'), may hold values from -0.4375 to 0.4375
- norm_gain: float32 [2048], replicated, may hold values from 0.1 to 1.9
- gate_weight: bfloat16 [2048, 3072], P('sp', 'tp'), may hold values from -0.125 to 0.125
- up_weight: bfloat16 [2048, 3072], P('sp', 'tp'), may hold values from -0.125 to 0.125
- down_weight: bfloat16 [3072, 2048], P('tp', 'sp'), may hold values from -0.21875 to 0.21875
Outputs:
- result: bfloat16 [2048, 2048], P(('sp', 'tp'))
All inputs are finite; a program needn't handle non-finite values.
Results may differ from a plain program's by a relative error of at most 0.028.
Values may be sent and summed in bfloat16 or wider, within the bound.
A program may use at most 64 MiB of HBM per device.

v0:
```python
import jax
import jax.numpy as jnp
from jax import lax
from jax.sharding import PartitionSpec as P

NARROW_SIZE = 64
BROAD_SIZE = 128


grain = 8
block_keys = 512
norm_eps = 1e-06


def block_plan(length):
    return (length // block_keys, block_keys)


def slice_rows(array, first, count):
    return lax.dynamic_slice_in_dim(array, first, count, 0)


def head_logs(queries, keys_block, offset_block, positions, key_positions, scale):
    logits = (
        jnp.einsum("qhd,khd->hqk", queries, keys_block, preferred_element_type=jnp.float32) * scale
    )
    logits = logits + jnp.transpose(offset_block)[:, None, :]
    causal = (key_positions[None, :] < positions[:, None])[None, :, :]
    lognot = jnp.where(causal, jax.nn.log_sigmoid(-logits), 0.0)
    return (logits, causal, lognot)


def sub_totals(lognot):
    heads, count, length = lognot.shape
    return lognot.reshape(heads, count, length // grain, grain).sum(axis=3)


def weighted_values(logits, causal, lognot, after, values):
    heads, count, length = lognot.shape
    grouped = lognot.reshape(heads, count, length // grain, grain)
    within = lax.cumsum(grouped, axis=3, reverse=True) - grouped
    later = (within + after[:, :, :, None]).reshape(heads, count, length)
    weights = jnp.where(causal, jnp.exp(jax.nn.log_sigmoid(logits) + later), 0.0).astype(
        jnp.bfloat16
    )
    return jnp.einsum("hqk,khd->qhd", weights, values, preferred_element_type=jnp.float32)


def local(
    stream,
    query_narrow,
    query_broad,
    key_narrow,
    key_broad,
    value_narrow,
    value_broad,
    key_offsets,
    out_narrow,
    out_broad,
    norm_gain,
    gate_weight,
    up_weight,
    down_weight,
):
    rows = stream.shape[0]
    heads = query_narrow.shape[1] // NARROW_SIZE
    shaped_narrow = query_narrow.reshape(rows, heads, NARROW_SIZE)
    shaped_broad = query_broad.reshape(rows, heads, BROAD_SIZE)
    positions = lax.axis_index("sp") * rows + jnp.arange(rows, dtype=jnp.int32)
    scale_narrow = NARROW_SIZE ** (-0.5)
    scale_broad = BROAD_SIZE ** (-0.5)

    def key_block(keys_narrow, keys_broad, offsets, first, count):
        block_narrow = slice_rows(keys_narrow, first, count).reshape(count, heads, NARROW_SIZE)
        block_broad = slice_rows(keys_broad, first, count).reshape(count, heads, BROAD_SIZE)
        pairs = slice_rows(offsets, first, count).reshape(count, heads, 2)
        return (block_narrow, block_broad, pairs[:, :, 0], pairs[:, :, 1])

    def value_block(values_narrow, values_broad, first, count):
        return (
            slice_rows(values_narrow, first, count).reshape(count, heads, NARROW_SIZE),
            slice_rows(values_broad, first, count).reshape(count, heads, BROAD_SIZE),
        )

    empty_narrow = jnp.zeros((rows, heads, NARROW_SIZE), jnp.float32)
    empty_broad = jnp.zeros((rows, heads, BROAD_SIZE), jnp.float32)
    total_subs = rows * lax.axis_size("sp") // grain
    zeros_subs = jnp.zeros((heads, rows, total_subs), jnp.float32)
    keys_narrow = lax.all_gather(key_narrow, "sp", axis=0, tiled=True)
    keys_broad = lax.all_gather(key_broad, "sp", axis=0, tiled=True)
    offsets = lax.all_gather(key_offsets.astype(jnp.bfloat16), "sp", axis=0, tiled=True).astype(
        jnp.float32
    )
    steps, span = block_plan(keys_narrow.shape[0])

    def count_one_step(index, sums):
        first = index * span
        block_narrow, block_broad, offset_narrow, offset_broad = key_block(
            keys_narrow, keys_broad, offsets, first, span
        )
        key_positions = first + jnp.arange(span, dtype=jnp.int32)
        slot = first // grain
        lognot_narrow = head_logs(
            shaped_narrow, block_narrow, offset_narrow, positions, key_positions, scale_narrow
        )[2]
        lognot_broad = head_logs(
            shaped_broad, block_broad, offset_broad, positions, key_positions, scale_broad
        )[2]
        return (
            lax.dynamic_update_slice(sums[0], sub_totals(lognot_narrow), (0, 0, slot)),
            lax.dynamic_update_slice(sums[1], sub_totals(lognot_broad), (0, 0, slot)),
        )

    sums_narrow, sums_broad = lax.fori_loop(0, steps, count_one_step, (zeros_subs, zeros_subs))
    after_narrow = lax.cumsum(sums_narrow, axis=2, reverse=True) - sums_narrow
    after_broad = lax.cumsum(sums_broad, axis=2, reverse=True) - sums_broad
    value_keys_narrow = lax.all_gather(key_narrow, "sp", axis=0, tiled=True)
    value_keys_broad = lax.all_gather(key_broad, "sp", axis=0, tiled=True)
    values_narrow = lax.all_gather(value_narrow, "sp", axis=0, tiled=True)
    values_broad = lax.all_gather(value_broad, "sp", axis=0, tiled=True)
    value_offsets = lax.all_gather(
        key_offsets.astype(jnp.bfloat16), "sp", axis=0, tiled=True
    ).astype(jnp.float32)
    steps, value_span = block_plan(value_keys_narrow.shape[0])

    def value_one_step(index, sums):
        first = index * value_span
        block_narrow, block_broad, offset_narrow, offset_broad = key_block(
            value_keys_narrow, value_keys_broad, value_offsets, first, value_span
        )
        held_narrow, held_broad = value_block(values_narrow, values_broad, first, value_span)
        key_positions = first + jnp.arange(value_span, dtype=jnp.int32)
        slot = first // grain
        logits_narrow, causal_narrow, lognot_narrow = head_logs(
            shaped_narrow, block_narrow, offset_narrow, positions, key_positions, scale_narrow
        )
        logits_broad, causal_broad, lognot_broad = head_logs(
            shaped_broad, block_broad, offset_broad, positions, key_positions, scale_broad
        )
        later_narrow = lax.dynamic_slice_in_dim(after_narrow, slot, value_span // grain, 2)
        later_broad = lax.dynamic_slice_in_dim(after_broad, slot, value_span // grain, 2)
        return (
            sums[0]
            + weighted_values(
                logits_narrow, causal_narrow, lognot_narrow, later_narrow, held_narrow
            ),
            sums[1]
            + weighted_values(logits_broad, causal_broad, lognot_broad, later_broad, held_broad),
        )

    acc_narrow, acc_broad = lax.fori_loop(0, steps, value_one_step, (empty_narrow, empty_broad))
    attended_narrow = acc_narrow.reshape(rows, heads * NARROW_SIZE).astype(jnp.bfloat16)
    attended_broad = acc_broad.reshape(rows, heads * BROAD_SIZE).astype(jnp.bfloat16)
    share = rows // lax.axis_size("tp")
    own = lax.axis_index("tp") * share
    first = jnp.int32(0)
    summed = lax.psum_scatter(
        (
            jnp.dot(
                slice_rows(attended_narrow, first, share * lax.axis_size("tp")),
                out_narrow,
                preferred_element_type=jnp.float32,
            )
            + jnp.dot(
                slice_rows(attended_broad, first, share * lax.axis_size("tp")),
                out_broad,
                preferred_element_type=jnp.float32,
            )
        ).astype(jnp.bfloat16),
        "tp",
        scatter_dimension=0,
        tiled=True,
    ).astype(jnp.float32)
    mid_own = (slice_rows(stream, own, share).astype(jnp.float32) + summed).astype(jnp.bfloat16)
    middle = mid_own.astype(jnp.float32)
    scaled = middle * lax.rsqrt(jnp.mean(middle * middle, axis=1, keepdims=True) + norm_eps)
    normed = lax.all_gather((scaled * norm_gain).astype(jnp.bfloat16), "tp", axis=0, tiled=True)
    part_gate = lax.all_gather(gate_weight, "sp", axis=0, tiled=True)
    part_up = lax.all_gather(up_weight, "sp", axis=0, tiled=True)
    gate = jnp.dot(normed, part_gate, preferred_element_type=jnp.float32)
    up = jnp.dot(normed, part_up, preferred_element_type=jnp.float32)
    hidden = (jax.nn.silu(gate) * up).astype(jnp.bfloat16)
    down_full = lax.all_gather(down_weight, "sp", axis=1, tiled=True)
    mixed = lax.psum_scatter(
        jnp.dot(
            slice_rows(hidden, jnp.int32(0), share * lax.axis_size("tp")),
            down_full,
            preferred_element_type=jnp.float32,
        ).astype(jnp.bfloat16),
        "tp",
        scatter_dimension=0,
        tiled=True,
    ).astype(jnp.float32)
    return (mid_own.astype(jnp.float32) + mixed).astype(jnp.bfloat16)


def solution(mesh):
    placed = (
        P("sp", None),
        P("sp", "tp"),
        P("sp", "tp"),
        P("sp", "tp"),
        P("sp", "tp"),
        P("sp", "tp"),
        P("sp", "tp"),
        P("sp", "tp"),
        P("tp", None),
        P("tp", None),
        P(),
        P("sp", "tp"),
        P("sp", "tp"),
        P("tp", "sp"),
    )
    return jax.shard_map(
        local, mesh=mesh, in_specs=placed, out_specs=P(("sp", "tp"), None), check_vma=False
    )
```

profile of v0, /device:TPU:0, one launch (start us, length us, event | category | flops | bytes accessed | tf_op | source)
XLA Modules:
  0.0 1451.3 jit_solution(2472093632499235351)
XLA Ops:
  15.9 43.0 %all_gather.32 = bf16[2048,8]{0,1:T(8,128)(2,1)S(1)} all-gather(bf16[128,8]{0,1:T(8,128)(2,1)S(1)} %convert_element_type.72), channel_id=1, replica_groups=mesh['sp'=16,'tp'=2] {'sp'}, dimensions={0}, use_global_device_ids=true | all-gather | bytes 34816 | tf_op jit(solution)/shard_map/all_gather | solution.py:121
  64.2 64.7 %all-gather.12.cloned.1.call-done = bf16[2048,512]{0,1:T(8,128)(2,1)} async-done(((bf16[128,512]{0,1:T(8,128)(2,1)}), bf16[2048,512]{0,1:T(8,128)(2,1)}) %all-gather.12.cloned.1.call-update) | async-done | bytes 2097168 | tf_op jit(solution)/shard_map/all_gather | solution.py:118
  129.0 28.6 %while.36 = (s32[]{:T(128)}, f32[4,128,256]{1,2,0:T(8,128)S(1)}, f32[4,128,256]{1,2,0:T(8,128)S(1)}, bf16[2048,256]{0,1:T(8,128)(2,1)}, bf16[128,4,64]{0,2,1:T(8...) while((s32[]{:T(128)}, f32[4,128,256]{1,2,0:T(8,128)S(1)}, ...), condition=%wide.region_3.4_spmd.clone, body=%wide.region_0.3_spmd.clone.sunk | while | flops 106431104 | bytes 3691926 | solution.py:114
  157.6 4.6 fusion.50
  165.1 4.6 fusion.48
  174.0 7.2 all-gather.8.cloned.1.call-done
  181.2 64.5 %all-gather.14.cloned.1.call-done = bf16[2048,512]{0,1:T(8,128)(2,1)} async-done(((bf16[128,512]{0,1:T(8,128)(2,1)}), bf16[2048,512]{0,1:T(8,128)(2,1)}) %all-gather.14.cloned.1.call-update) | async-done | bytes 2097168 | tf_op jit(solution)/shard_map/all_gather | solution.py:120
  245.8 863.7 %while.37 = (s32[]{:T(128)}, f32[128,4,64]{0,2,1:T(8,128)}, f32[128,4,128]{0,2,1:T(8,128)}, bf16[2048,256]{0,1:T(8,128)(2,1)}, bf16[2048,256]{0,1:T(8,128)(2,1)}...) while((s32[]{:T(128)}, f32[128,4,64]{0,2,1:T(8,128)}, ...), condition=%wide.region_11.12_spmd.clone, body=%wide.region_8.11_spmd.clone.sunk | while | flops 221512320 | bytes 29971964 | solution.py:151
  273.9 96.6 %reduce_window_sum.71 = f32[4,128,64,8]{1,3,2,0:T(8,128)} reduce-window(f32[4,128,64,8]{1,3,2,0:T(8,128)} %get-tuple-element.879, f32[]{:T(128)} %constant.262.clone.1..sunk), window={size=1x1x1x8 pad=0_0x0_0x0_0x0_7}, to_apply=%region_10.10 | reduce-window | flops 1835008 | bytes 2097156 | tf_op jit(solution)/shard_map/while/body/eval_jaxpr/reduce_window_sum | solution.py:41
  376.3 95.5 %reduce_window_sum.70 = f32[4,128,64,8]{1,3,2,0:T(8,128)} reduce-window(f32[4,128,64,8]{1,3,2,0:T(8,128)S(1)} %get-tuple-element.876, f32[]{:T(128)} %constant.262.clone.1..sunk), window={size=1x1x1x8 pad=0_0x0_0x0_0x0_7}, to_apply=%region_9.9 | reduce-window | flops 1835008 | bytes 2097156 | tf_op jit(solution)/shard_map/while/body/eval_jaxpr/reduce_window_sum | solution.py:41
  485.0 96.6 %reduce_window_sum.71 = f32[4,128,64,8]{1,3,2,0:T(8,128)} reduce-window(f32[4,128,64,8]{1,3,2,0:T(8,128)} %get-tuple-element.879, f32[]{:T(128)} %constant.262.clone.1..sunk), window={size=1x1x1x8 pad=0_0x0_0x0_0x0_7}, to_apply=%region_10.10 | reduce-window | flops 1835008 | bytes 2097156 | tf_op jit(solution)/shard_map/while/body/eval_jaxpr/reduce_window_sum | solution.py:41
  587.4 95.5 %reduce_window_sum.70 = f32[4,128,64,8]{1,3,2,0:T(8,128)} reduce-window(f32[4,128,64,8]{1,3,2,0:T(8,128)S(1)} %get-tuple-element.876, f32[]{:T(128)} %constant.262.clone.1..sunk), window={size=1x1x1x8 pad=0_0x0_0x0_0x0_7}, to_apply=%region_9.9 | reduce-window | flops 1835008 | bytes 2097156 | tf_op jit(solution)/shard_map/while/body/eval_jaxpr/reduce_window_sum | solution.py:41
  696.2 96.6 %reduce_window_sum.71 = f32[4,128,64,8]{1,3,2,0:T(8,128)} reduce-window(f32[4,128,64,8]{1,3,2,0:T(8,128)} %get-tuple-element.879, f32[]{:T(128)} %constant.262.clone.1..sunk), window={size=1x1x1x8 pad=0_0x0_0x0_0x0_7}, to_apply=%region_10.10 | reduce-window | flops 1835008 | bytes 2097156 | tf_op jit(solution)/shard_map/while/body/eval_jaxpr/reduce_window_sum | solution.py:41
  794.5 4.2 fusion.118
  798.7 95.5 %reduce_window_sum.70 = f32[4,128,64,8]{1,3,2,0:T(8,128)} reduce-window(f32[4,128,64,8]{1,3,2,0:T(8,128)S(1)} %get-tuple-element.876, f32[]{:T(128)} %constant.262.clone.1..sunk), window={size=1x1x1x8 pad=0_0x0_0x0_0x0_7}, to_apply=%region_9.9 | reduce-window | flops 1835008 | bytes 2097156 | tf_op jit(solution)/shard_map/while/body/eval_jaxpr/reduce_window_sum | solution.py:41
  907.5 96.6 %reduce_window_sum.71 = f32[4,128,64,8]{1,3,2,0:T(8,128)} reduce-window(f32[4,128,64,8]{1,3,2,0:T(8,128)} %get-tuple-element.879, f32[]{:T(128)} %constant.262.clone.1..sunk), window={size=1x1x1x8 pad=0_0x0_0x0_0x0_7}, to_apply=%region_10.10 | reduce-window | flops 1835008 | bytes 2097156 | tf_op jit(solution)/shard_map/while/body/eval_jaxpr/reduce_window_sum | solution.py:41
  1005.7 4.1 fusion.118
  1009.9 95.5 %reduce_window_sum.70 = f32[4,128,64,8]{1,3,2,0:T(8,128)} reduce-window(f32[4,128,64,8]{1,3,2,0:T(8,128)S(1)} %get-tuple-element.876, f32[]{:T(128)} %constant.262.clone.1..sunk), window={size=1x1x1x8 pad=0_0x0_0x0_0x0_7}, to_apply=%region_9.9 | reduce-window | flops 1835008 | bytes 2097156 | tf_op jit(solution)/shard_map/while/body/eval_jaxpr/reduce_window_sum | solution.py:41
  1124.0 93.7 %all-gather.16.cloned.1.call-done = bf16[2048,1536]{1,0:T(8,128)(2,1)} async-done(((bf16[128,1536]{1,0:T(8,128)(2,1)}), bf16[2048,1536]{1,0:T(8,128)(2,1)}) %all-gather.16.cloned.1.call-update) | async-done | bytes 6291472 | tf_op jit(solution)/shard_map/all_gather | solution.py:178
  1217.7 4.7 fusion.57
  1222.4 90.1 %all-gather.18.cloned.1.call-done = bf16[2048,1536]{1,0:T(8,128)(2,1)} async-done(((bf16[128,1536]{1,0:T(8,128)(2,1)}), bf16[2048,1536]{1,0:T(8,128)(2,1)}) %all-gather.18.cloned.1.call-update) | async-done | bytes 6291472 | tf_op jit(solution)/shard_map/all_gather | solution.py:179
  1312.5 116.3 %all-gather.20.cloned.1.call-done = bf16[1536,2048]{1,0:T(8,128)(2,1)} async-done(((bf16[1536,128]{1,0:T(8,128)(2,1)}), bf16[1536,2048]{1,0:T(8,128)(2,1)}) %all-gather.20.cloned.1.call-update) | async-done | bytes 6291472 | tf_op jit(solution)/shard_map/all_gather | solution.py:183
  1428.8 7.7 convolution_convert_fusion
  1436.5 6.3 reduce-scatter.5.cloned.1.call-done
  (189 shorter events, 133.9 us)
Async XLA Ops:
  6.5 1106.4 %copy-start = (bf16[512,2048]{1,0:T(8,128)(2,1)S(1)}, bf16[512,2048]{1,0:T(8,128)(2,1)}, u32[]{:S(2)}) copy-start(bf16[512,2048]{1,0:T(8,128)(2,1)} %param.27) | copy-start | bytes 6291460
  6.5 57.7 %all-gather.10.cloned.1.call-start = ((), (), s32[]{:S(2)}) async-start(), calls=%async_computation.3 | async-start | bytes 1114112 | tf_op jit(solution)/shard_map/all_gather | solution.py:117
  8.3 120.6 %all-gather.12.cloned.1.call-start = ((), (), s32[]{:S(2)}) async-start(), calls=%async_computation.4 | async-start | bytes 2228224 | tf_op jit(solution)/shard_map/all_gather | solution.py:118
  10.0 171.2 %all-gather.8.cloned.1.call-start = ((), (), s32[]{:S(2)}) async-start(), calls=%async_computation.2 | async-start | bytes 1114112 | tf_op jit(solution)/shard_map/all_gather | solution.py:119
  11.6 234.1 %all-gather.14.cloned.1.call-start = ((), (), s32[]{:S(2)}) async-start(), calls=%async_computation.5 | async-start | bytes 2228224 | tf_op jit(solution)/shard_map/all_gather | solution.py:120
  13.4 1107.2 %reduce-scatter.3.cloned.1.call-start = ((), (), s32[]{:S(2)}) async-start(), calls=%async_computation.6 | async-start | bytes 786432 | tf_op jit(solution)/shard_map/reduce_scatter | solution.py:157
  162.2 0.8 copy-start.3
  169.7 0.8 copy-start.4
  268.8 5.2 copy-start.2
  270.7 1.0 copy-start.1
  479.9 5.2 copy-start.2
  481.8 1.0 copy-start.1
  691.1 5.2 copy-start.2
  693.0 1.0 copy-start.1
  902.3 5.2 copy-start.2
  904.3 1.0 copy-start.1
  1109.4 11.1 copy-start.5
  1109.4 12.3 copy-start.6
  1114.3 103.5 %all-gather.16.cloned.1.call-start = ((), (), s32[]{:S(2)}) async-start(), calls=%async_computation.7 | async-start | bytes 6684672 | tf_op jit(solution)/shard_map/all_gather | solution.py:178
  1114.8 197.6 %all-gather.18.cloned.1.call-start = ((), (), s32[]{:S(2)}) async-start(), calls=%async_computation.8 | async-start | bytes 6684672 | tf_op jit(solution)/shard_map/all_gather | solution.py:179
  1115.6 313.2 %all-gather.20.cloned.1.call-start = ((), (), s32[]{:S(2)}) async-start(), calls=%async_computation.9 | async-start | bytes 6684672 | tf_op jit(solution)/shard_map/all_gather | solution.py:183
  1116.3 326.4 %reduce-scatter.5.cloned.1.call-start = ((), (), s32[]{:S(2)}) async-start(), calls=%async_computation.10 | async-start | bytes 786432 | tf_op jit(solution)/shard_map/reduce_scatter | solution.py:184
Sparse Core Ops, SparseCore 0:
  10.0 54.1 all-gather.9
  66.9 61.9 all-gather.11
  131.6 49.5 all-gather.7
  183.8 61.9 all-gather.13
  1114.4 6.0 reduce-scatter.2
  1123.2 94.5 all-gather.15
  1220.5 91.9 all-gather.17
  1315.2 113.5 all-gather.19
  1436.6 6.0 reduce-scatter.4
where the time goes:
time: 1460 us; the launch traced here: 1450 us
  other arithmetic  798 us (55%)
  waiting for transfers between devices  453 us (31%)
  matrix products  67.9 us (5%)
  local copies, waits for them, and re-layouts  53.3 us (4%)
  blocking collectives  45.2 us (3%)
  loops' own time  20 us (1%)
    another operation x8, other arithmetic, weighted_values(): within = lax.cumsum(grouped, axis=3, reverse=True) - grouped  768 us
    all_gather x1, waiting for transfers between devices, local(): down_full = lax.all_gather(down_weight, 'sp', axis=1, tiled=True)  116 us
    all_gather x1, waiting for transfers between devices, local(): part_gate = lax.all_gather(gate_weight, 'sp', axis=0, tiled=True)  93.7 us
    all_gather x1, waiting for transfers between devices, local(): part_up = lax.all_gather(up_weight, 'sp', axis=0, tiled=True)  90.1 us
    all_gather x1, waiting for transfers between devices, local(): value_keys_broad = lax.all_gather(key_broad, 'sp', axis=0, tiled=True)  64.7 us
    all_gather x1, waiting for transfers between devices, local(): values_broad = lax.all_gather(value_broad, 'sp', axis=0, tiled=True)  64.5 us
    all_gather x1, blocking collectives, local(): lax.all_gather(key_offsets.astype(jnp.bfloat16), 'sp', axis=0, tiled=True)  43 us
    dot_general x8, matrix products, weighted_values(): jnp.einsum('hqk,khd->qhd', weights, values, preferred_element_type=jnp.fl...  31.9 us
  transfers between devices with their start and end apart: 9, of which 9 were waited for; matrix products, arithmetic and copies ran while one was open for 4% of the time, Pallas kernels for 0%

commit v1 on v0

v1 whole, which is shorter than its diff:
```python
import functools

import jax
import jax.numpy as jnp
from jax import lax
from jax.experimental import pallas as pl
from jax.experimental.pallas import tpu as pltpu
from jax.sharding import PartitionSpec as P

NARROW_SIZE = 64
BROAD_SIZE = 128
WIDE = 128
norm_eps = 1e-06
MESH = pl.DeviceIdType.MESH


def greet(axis_peers):
    barrier = pltpu.get_barrier_semaphore()
    count = 0
    for peers, total in axis_peers:
        def signal(t, carry, peers=peers):
            pl.semaphore_signal(barrier, inc=1, device_id=peers(t), device_id_type=MESH)
            return carry

        lax.fori_loop(1, total, signal, 0)
        count += total - 1
    pl.semaphore_wait(barrier, count)


def attend_kernel(n, hp, rows, group, q_ref, kv_ref, off_ref, *rest):
    H = 2 * hp
    R = n // H
    weights_too = group > 0
    if weights_too:
        (gate_ref, up_ref, down_ref, att_ref, gate_all, up_all, down_all) = rest[:7]
        rest = rest[7:]
    else:
        att_ref = rest[0]
        rest = rest[1:]
    (kvbuf, offbuf, qbuf, obuf, tri, kv_s, kv_r, off_s, off_r, q_s, q_r, att_s, att_r) = rest[:13]
    me = lax.axis_index("sp")
    head = me // R
    sub = me % R

    def snake(b):
        v = b % (2 * R)
        return jnp.where(v < R, v, 2 * R - 1 - v)

    def block_of(i, r):
        return i * R + jnp.where(i % 2 == 0, r, R - 1 - r)

    def peer(t):
        return lax.rem(me + t, n)

    def kv_copy(d, slot_src, sem):
        return pltpu.make_async_remote_copy(
            src_ref=kv_ref.at[d // R], dst_ref=kvbuf.at[slot_src], send_sem=kv_s.at[sem],
            recv_sem=kv_r.at[slot_src], device_id={"sp": d}, device_id_type=MESH)

    def off_copy(d, slot_src, sem):
        return pltpu.make_async_remote_copy(
            src_ref=off_ref.at[d // R], dst_ref=offbuf.at[slot_src], send_sem=off_s.at[sem],
            recv_sem=off_r.at[slot_src], device_id={"sp": d}, device_id_type=MESH)

    def q_copy(h, d, slot):
        return pltpu.make_async_remote_copy(
            src_ref=q_ref.at[h], dst_ref=qbuf.at[slot], send_sem=q_s.at[h],
            recv_sem=q_r.at[slot], device_id={"sp": d}, device_id_type=MESH)

    def att_copy(i, d, h):
        return pltpu.make_async_remote_copy(
            src_ref=obuf.at[i], dst_ref=att_ref.at[h], send_sem=att_s.at[i],
            recv_sem=att_r.at[h], device_id={"sp": d}, device_id_type=MESH)

    if weights_too:
        (g_s, g_r, u_s, u_r, d_s, d_r) = rest[13:19]
        drows = gate_ref.shape[0]
        fcols = gate_all.shape[1]
        dcols = down_ref.shape[1]

        def w_pieces(d, src):
            part = pl.multiple_of((d % group) * fcols, 128)
            at_rows = pl.ds(pl.multiple_of(src * drows, 128), drows)
            at_cols = pl.ds(pl.multiple_of(src * dcols, 128), dcols)
            return (
                (gate_ref.at[:, pl.ds(part, fcols)], gate_all.at[at_rows, :], g_s, g_r),
                (up_ref.at[:, pl.ds(part, fcols)], up_all.at[at_rows, :], u_s, u_r),
                (down_ref.at[pl.ds(part, fcols), :], down_all.at[:, at_cols], d_s, d_r),
            )

        def w_copies(d, src, sem):
            return [
                pltpu.make_async_remote_copy(
                    src_ref=a, dst_ref=b, send_sem=ss.at[sem], recv_sem=rs.at[src],
                    device_id={"sp": d}, device_id_type=MESH)
                for a, b, ss, rs in w_pieces(d, src)
            ]

        def w_local():
            return [pltpu.make_async_copy(a, b, rs.at[me]) for a, b, ss, rs in w_pieces(me, me)]

    greet([(lambda t: {"sp": peer(t)}, n)])

    def send_q(h, carry):
        d = h * R + snake(me)

        @pl.when(d != me)
        def _():
            q_copy(h, d, me // R).start()

        @pl.when(d == me)
        def _():
            pltpu.make_async_copy(q_ref.at[h], qbuf.at[me // R], q_r.at[me // R]).start()

        return carry

    def send_kv(t, carry):
        d = peer(t)
        kv_copy(d, me, t).start()
        off_copy(d, me, t).start()
        return carry

    lax.fori_loop(1, n, send_kv, 0)
    lax.fori_loop(0, H, send_q, 0)
    pltpu.make_async_copy(kv_ref.at[head], kvbuf.at[me], kv_r.at[me]).start()
    pltpu.make_async_copy(off_ref.at[head], offbuf.at[me], off_r.at[me]).start()
    if weights_too:
        def send_w(t, carry):
            for c in w_copies(peer(t), me, t):
                c.start()
            return carry

        lax.fori_loop(1, n, send_w, 0)
        for c in w_local():
            c.start()

    row = lax.broadcasted_iota(jnp.int32, (WIDE, WIDE), 0)
    col = lax.broadcasted_iota(jnp.int32, (WIDE, WIDE), 1)
    strict = jnp.where(row > col, 1.0, 0.0).astype(jnp.bfloat16)
    ones = jnp.ones((WIDE, WIDE), jnp.bfloat16)
    half = jnp.concatenate([strict, ones], axis=1)
    tri[...] = jnp.concatenate([half, half], axis=0)

    def wait_kv(t, carry):
        src = peer(t)
        kv_copy(src, src, t).wait_recv()
        off_copy(src, src, t).wait_recv()
        return carry

    lax.fori_loop(1, n, wait_kv, 0)
    pltpu.make_async_copy(kv_ref.at[head], kvbuf.at[me], kv_r.at[me]).wait()
    pltpu.make_async_copy(off_ref.at[head], offbuf.at[me], off_r.at[me]).wait()

    scale = jnp.where(head < hp, jnp.float32(NARROW_SIZE ** (-0.5)), jnp.float32(BROAD_SIZE ** (-0.5)))
    wide = 4 if n % 4 == 0 else 1

    def one_query(i, carry):
        b = block_of(i, sub)

        @pl.when(b != me)
        def _():
            q_copy(head, b, i).wait_recv()

        @pl.when(b == me)
        def _():
            pltpu.make_async_copy(q_ref.at[head], qbuf.at[i], q_r.at[i]).wait()

        q = qbuf[i]
        chunks = b // wide + 1

        def one_chunk(step, state):
            acc, later = state
            c = chunks - 1 - step
            held = kvbuf[pl.ds(c * wide, wide)]
            pieces = [None] * wide
            for k in reversed(range(wide)):
                logits = lax.dot_general(
                    q, held[k, 0], (((1,), (1,)), ((), ())), preferred_element_type=jnp.float32
                ) * scale + offbuf[c * wide + k][0:1, :]
                causal = (c * wide + k) * rows + col < b * rows + row
                soft = jnp.maximum(logits, 0.0) + jnp.log(1.0 + jnp.exp(-jnp.abs(logits)))
                masked = jnp.where(causal, soft, 0.0)
                high = masked.astype(jnp.bfloat16)
                low = (masked - high.astype(jnp.float32)).astype(jnp.bfloat16)
                sums = jnp.dot(
                    jnp.concatenate([high, low], axis=1), tri[...], preferred_element_type=jnp.float32
                )
                exponent = (logits - soft) - (sums[:, :WIDE] + later)
                pieces[k] = jnp.where(causal, jnp.exp(exponent), 0.0).astype(jnp.bfloat16)
                later = later + sums[:, WIDE:]
            weights = jnp.concatenate(pieces, axis=1)
            values = held[:, 1].reshape(wide * rows, WIDE)
            acc = acc + jnp.dot(weights, values, preferred_element_type=jnp.float32)
            return acc, later

        zero = jnp.zeros((rows, WIDE), jnp.float32)
        acc, _ = lax.fori_loop(0, chunks, one_chunk, (zero, zero))
        obuf[i] = acc.astype(jnp.bfloat16)

        @pl.when(b != me)
        def _():
            att_copy(i, b, head).start()

        @pl.when(b == me)
        def _():
            pltpu.make_async_copy(obuf.at[i], att_ref.at[head], att_r.at[head]).start()

        return carry

    lax.fori_loop(0, H, one_query, 0)

    def wait_sends(t, carry):
        d = peer(t)
        kv_copy(d, me, t).wait_send()
        off_copy(d, me, t).wait_send()
        if weights_too:
            for c in w_copies(d, me, t):
                c.wait_send()
            for c in w_copies(d, d, t):
                c.wait_recv()
        return carry

    lax.fori_loop(1, n, wait_sends, 0)
    if weights_too:
        for c in w_local():
            c.wait()

    def wait_att(h, carry):
        d = h * R + snake(me)
        b = block_of(h, sub)

        @pl.when(d != me)
        def _():
            q_copy(h, d, me // R).wait_send()
            att_copy(0, d, h).wait_recv()

        @pl.when(d == me)
        def _():
            pltpu.make_async_copy(obuf.at[0], att_ref.at[h], att_r.at[h]).wait()

        @pl.when(b != me)
        def _():
            att_copy(h, b, head).wait_send()

        return carry

    lax.fori_loop(0, H, wait_att, 0)


def attend(n, hp, rows, group, q, kv, off, weights):
    H = 2 * hp
    dma = pltpu.SemaphoreType.DMA
    vmem = pl.BlockSpec(memory_space=pltpu.VMEM)
    hbm = pl.BlockSpec(memory_space=pl.ANY)
    out_shape = [jax.ShapeDtypeStruct((H, rows, WIDE), jnp.bfloat16)]
    scratch = [
        pltpu.VMEM((n, 2, rows, WIDE), jnp.bfloat16),
        pltpu.VMEM((n, 8, WIDE), jnp.float32),
        pltpu.VMEM((H, rows, WIDE), jnp.bfloat16),
        pltpu.VMEM((H, rows, WIDE), jnp.bfloat16),
        pltpu.VMEM((2 * WIDE, 2 * WIDE), jnp.bfloat16),
        dma((n,)), dma((n,)), dma((n,)), dma((n,)), dma((H,)), dma((H,)), dma((H,)), dma((H,)),
    ]
    args = [q, kv, off]
    specs = [vmem] * 3
    if group:
        gate, up, down = weights
        cols = gate.shape[1] // group
        out_shape += [jax.ShapeDtypeStruct((gate.shape[0] * n, cols), jnp.bfloat16)] * 2
        out_shape += [jax.ShapeDtypeStruct((cols, down.shape[1] * n), jnp.bfloat16)]
        scratch += [dma((n,))] * 6
        args += [gate, up, down]
        specs += [hbm] * 3
    return pl.pallas_call(
        functools.partial(attend_kernel, n, hp, rows, group),
        out_shape=out_shape,
        in_specs=specs,
        out_specs=[hbm] * len(out_shape),
        scratch_shapes=scratch,
        compiler_params=pltpu.CompilerParams(
            collective_id=0, has_side_effects=True, vmem_limit_bytes=40 * 1024 * 1024
        ),
    )(*args)


def mix_kernel(a, T, hp, att_ref, on_ref, ob_ref, stream_ref, gain_ref, gate_ref, up_ref, down_ref,
               out_ref, pbuf, prec, mid, xs, pb, ps, p_s, p_r, x_s, x_r, r_s, r_r):
    G = a * T
    me = lax.axis_index("sp")
    j = lax.axis_index("tp")
    base = (me // a) * a
    g = (me - base) * T + j
    share = out_ref.shape[0]

    def place(e):
        return {"sp": base + e // T, "tp": e % T}

    def other(t):
        return lax.rem(g + t, G)

    greet([(lambda t: place(other(t)), G)])

    cut = [att_ref[h][:, :NARROW_SIZE] for h in range(hp)]
    part = jnp.dot(jnp.concatenate(cut, axis=1), on_ref[...], preferred_element_type=jnp.float32)
    part = part + jnp.dot(
        jnp.concatenate([att_ref[hp + h] for h in range(hp)], axis=1), ob_ref[...],
        preferred_element_type=jnp.float32,
    )
    pbuf[...] = part.astype(jnp.bfloat16).reshape(pbuf.shape)

    def p_copy(to, src, t):
        return pltpu.make_async_remote_copy(
            src_ref=pbuf.at[to], dst_ref=prec.at[src], send_sem=p_s.at[t], recv_sem=p_r.at[src],
            device_id={"tp": to}, device_id_type=MESH)

    for t in range(1, T):
        p_copy(lax.rem(j + t, T), j, t).start()
    total = pbuf[j].astype(jnp.float32)
    for t in range(1, T):
        src = lax.rem(j + t, T)
        p_copy(src, src, t).wait_recv()
        total = total + prec[src].astype(jnp.float32)
    own = pl.ds(pl.multiple_of(j * share, share), share)
    mid[...] = (stream_ref[own, :].astype(jnp.float32) + total).astype(jnp.bfloat16)
    middle = mid[...].astype(jnp.float32)
    scaled = middle * lax.rsqrt(jnp.mean(middle * middle, axis=1, keepdims=True) + norm_eps)
    xs[g] = (scaled * gain_ref[...]).astype(jnp.bfloat16)

    def x_copy(e, src, t):
        return pltpu.make_async_remote_copy(
            src_ref=xs.at[src], dst_ref=xs.at[src], send_sem=x_s.at[t], recv_sem=x_r.at[src],
            device_id=place(e), device_id_type=MESH)

    def r_copy(e, src):
        return pltpu.make_async_remote_copy(
            src_ref=pb.at[e], dst_ref=ps.at[src], send_sem=r_s.at[e], recv_sem=r_r.at[src],
            device_id=place(e), device_id_type=MESH)

    def send_x(t, carry):
        x_copy(other(t), g, t).start()
        return carry

    lax.fori_loop(1, G, send_x, 0)

    def one_member(k, carry):
        m = lax.rem(me - base + k, a)
        for s in range(T):
            e = m * T + s

            @pl.when(e != g)
            def _():
                x_copy(e, e, 0).wait_recv()

        x = xs[pl.ds(m * T, T)].reshape(T * share, xs.shape[2])
        gate = jnp.dot(x, gate_ref[...], preferred_element_type=jnp.float32)
        up = jnp.dot(x, up_ref[...], preferred_element_type=jnp.float32)
        hidden = (gate / (1.0 + jnp.exp(-gate)) * up).astype(jnp.bfloat16)
        mixed = jnp.dot(hidden, down_ref[...], preferred_element_type=jnp.float32)
        pb[pl.ds(m * T, T)] = mixed.astype(jnp.bfloat16).reshape(T, share, mixed.shape[1])
        for s in range(T):
            e = m * T + s

            @pl.when(e != g)
            def _():
                r_copy(e, g).start()

        return carry

    lax.fori_loop(0, a, one_member, 0)
    total = pb[g].astype(jnp.float32)
    for t in range(1, G):
        e = other(t)
        r_copy(e, e).wait_recv()
        total = total + ps[e].astype(jnp.float32)
    out_ref[...] = (mid[...].astype(jnp.float32) + total).astype(jnp.bfloat16)
    for t in range(1, T):
        p_copy(lax.rem(j + t, T), j, t).wait_send()

    def finish(t, carry):
        x_copy(other(t), g, t).wait_send()
        r_copy(other(t), g).wait_send()
        return carry

    lax.fori_loop(1, G, finish, 0)


def mix(a, T, hp, att, out_narrow, out_broad, stream, gain, gate, up, down):
    G = a * T
    rows, width = stream.shape
    share = rows // T
    dma = pltpu.SemaphoreType.DMA
    block = pltpu.VMEM((G, share, width), jnp.bfloat16)
    pair = pltpu.VMEM((T, share, width), jnp.bfloat16)
    return pl.pallas_call(
        functools.partial(mix_kernel, a, T, hp),
        out_shape=jax.ShapeDtypeStruct((share, width), jnp.bfloat16),
        in_specs=[pl.BlockSpec(memory_space=pltpu.VMEM)] * 8,
        out_specs=pl.BlockSpec(memory_space=pltpu.VMEM),
        scratch_shapes=[
            pair, pair, pltpu.VMEM((share, width), jnp.bfloat16), block, block, block,
            dma((T,)), dma((T,)), dma((G,)), dma((G,)), dma((G,)), dma((G,)),
        ],
        compiler_params=pltpu.CompilerParams(
            collective_id=1, has_side_effects=True, vmem_limit_bytes=60 * 1024 * 1024
        ),
    )(att, out_narrow, out_broad, stream, gain.reshape(1, width), gate, up, down)


def split_heads(array, heads, size):
    cut = jnp.transpose(array.reshape(array.shape[0], heads, size), (1, 0, 2))
    return jnp.pad(cut, ((0, 0), (0, 0), (0, WIDE - size)))


def local(n, T,
    stream,
    query_narrow,
    query_broad,
    key_narrow,
    key_broad,
    value_narrow,
    value_broad,
    key_offsets,
    out_narrow,
    out_broad,
    norm_gain,
    gate_weight,
    up_weight,
    down_weight,
):
    rows = stream.shape[0]
    hp = query_narrow.shape[1] // NARROW_SIZE

    def both(narrow, broad):
        return jnp.concatenate(
            [split_heads(narrow, hp, NARROW_SIZE), split_heads(broad, hp, BROAD_SIZE)], axis=0
        )

    q = both(query_narrow, query_broad)
    kv = jnp.stack([both(key_narrow, key_broad), both(value_narrow, value_broad)], axis=1)
    off = jnp.transpose(jnp.concatenate([key_offsets[:, 0::2], key_offsets[:, 1::2]], axis=1))
    off = jnp.broadcast_to(off[:, None, :], (2 * hp, 8, rows))
    group = 0
    if gate_weight.shape[0] % 128 == 0 and down_weight.shape[1] % 128 == 0:
        for a in (1, 2, 4):
            if n % a == 0 and gate_weight.shape[1] % (128 * a) == 0:
                group = a
    if group:
        att, gate_all, up_all, down_all = attend(
            n, hp, rows, group, q, kv, off, (gate_weight, up_weight, down_weight)
        )
        return mix(
            group, T, hp, att, out_narrow, out_broad, stream, norm_gain, gate_all, up_all, down_all
        )
    att = attend(n, hp, rows, 0, q, kv, off, None)[0]
    attended_narrow = jnp.transpose(att[:hp, :, :NARROW_SIZE], (1, 0, 2)).reshape(rows, -1)
    attended_broad = jnp.transpose(att[hp:], (1, 0, 2)).reshape(rows, -1)
    share = rows // T
    own = lax.axis_index("tp") * share
    summed = lax.psum_scatter(
        (
            jnp.dot(attended_narrow, out_narrow, preferred_element_type=jnp.float32)
            + jnp.dot(attended_broad, out_broad, preferred_element_type=jnp.float32)
        ).astype(jnp.bfloat16),
        "tp",
        scatter_dimension=0,
        tiled=True,
    ).astype(jnp.float32)
    mid_own = (lax.dynamic_slice_in_dim(stream, own, share, 0).astype(jnp.float32) + summed).astype(
        jnp.bfloat16
    )
    middle = mid_own.astype(jnp.float32)
    scaled = middle * lax.rsqrt(jnp.mean(middle * middle, axis=1, keepdims=True) + norm_eps)
    normed = lax.all_gather((scaled * norm_gain).astype(jnp.bfloat16), "tp", axis=0, tiled=True)
    part_gate = lax.all_gather(gate_weight, "sp", axis=0, tiled=True)
    part_up = lax.all_gather(up_weight, "sp", axis=0, tiled=True)
    gate = jnp.dot(normed, part_gate, preferred_element_type=jnp.float32)
    up = jnp.dot(normed, part_up, preferred_element_type=jnp.float32)
    hidden = (jax.nn.silu(gate) * up).astype(jnp.bfloat16)
    down_full = lax.all_gather(down_weight, "sp", axis=1, tiled=True)
    mixed = lax.psum_scatter(
        jnp.dot(
            hidden,
            down_full,
            preferred_element_type=jnp.float32,
        ).astype(jnp.bfloat16),
        "tp",
        scatter_dimension=0,
        tiled=True,
    ).astype(jnp.float32)
    return (mid_own.astype(jnp.float32) + mixed).astype(jnp.bfloat16)


def solution(mesh):
    placed = (
        P("sp", None),
        P("sp", "tp"),
        P("sp", "tp"),
        P("sp", "tp"),
        P("sp", "tp"),
        P("sp", "tp"),
        P("sp", "tp"),
        P("sp", "tp"),
        P("tp", None),
        P("tp", None),
        P(),
        P("sp", "tp"),
        P("sp", "tp"),
        P("tp", "sp"),
    )
    body = functools.partial(local, mesh.shape["sp"], mesh.shape["tp"])
    return jax.shard_map(
        body, mesh=mesh, in_specs=placed, out_specs=P(("sp", "tp"), None), check_vma=False
    )
```

time: 1460 us -> 227 us (0.16)
  other arithmetic: 798 us -> 0.16 us
  waiting for transfers between devices: 453 us -> 0 us
  Pallas kernels: 0 us -> 212 us
  matrix products: 67.9 us -> 0 us
  blocking collectives: 45.2 us -> 0 us
  local copies, waits for them, and re-layouts: 53.3 us -> 12.8 us
  loops' own time: 20 us -> 0 us
    another operation x14 -> x2, other arithmetic: 780 us -> 0.12 us  [local(): jnp.stack([both(key_narrow, key_broad), both(value_narrow, value_broad)],...]
    all_gather x7 -> x0, waiting for transfers between devices: 440 us -> none  [the longest x1 116 us: local(): down_full = lax.all_gather(down_weight, 'sp', axis=1, tiled=True)]
    pallas_call x0 -> x2, Pallas kernels: none -> 212 us  [the longest x1 158 us: attend(): pl.pallas_call(functools.partial(attend_kernel, n, hp, rows, group), out_...]
    dot_general x28 -> x0, matrix products: 67.9 us -> none  [the longest x8 31.9 us: weighted_values(): jnp.einsum('hqk,khd->qhd', weights, values, preferred_element_type=jnp.fl...]
    all_gather x2 -> x0, blocking collectives: 45.2 us -> none  [the longest x1 43 us: local(): lax.all_gather(key_offsets.astype(jnp.bfloat16), 'sp', axis=0, tiled=True)]
    dynamic_slice x28 -> x0, local copies, waits for them, and re-layouts: 35 us -> none  [the longest x24 28.2 us: slice_rows(): return lax.dynamic_slice_in_dim(array, first, count, 0)]
    another operation x2 -> x0, loops' own time: 20 us -> none  [the longest x1 19.2 us: local(): lax.fori_loop(0, steps, value_one_step, (empty_narrow, empty_broad))]
  transfers between devices with their start and end apart: 9 -> 0, of which waited for: 9 -> 0; matrix products, arithmetic and copies ran while one was open for 4% -> 0% of each run, Pallas kernels for 0% -> 0%
where the time goes in v1:
time: 227 us; the launch traced here: 226 us
  Pallas kernels  212 us (93%)
  local copies, waits for them, and re-layouts  12.8 us (6%)
    pallas_call x1, Pallas kernels, attend(): pl.pallas_call(functools.partial(attend_kernel, n, hp, rows, group), out_...  158 us
    pallas_call x1, Pallas kernels, mix(): pl.pallas_call(functools.partial(mix_kernel, a, T, hp), out_shape=jax.Sha...  54.3 us
    unnamed x25, local copies, waits for them, and re-layouts  10.5 us

profile of v1, /device:TPU:0, one launch (start us, length us, event | category | flops | bytes accessed | tf_op | source)
XLA Modules:
  0.0 225.5 jit_solution(3869186013139437329)
XLA Ops:
  0.0 0.7 slice.7
  0.7 0.7 slice.6
  1.5 0.9 copy.15
  2.4 0.1 copy.16
  2.6 1.0 copy.19
  3.5 0.1 copy.20
  3.7 1.0 copy.23
  4.6 0.1 copy.24
  4.8 1.0 copy.17
  5.8 0.1 copy.18
  6.0 0.1 copy.21
  6.1 0.1 copy.22
  6.3 0.1 copy.25
  6.4 0.1 copy.26
  6.7 0.3 copy-done.3
  7.0 0.1 copy-done.4
  7.1 0.1 copy-done.5
  7.2 158.2 %shard_map.136 = (bf16[8,128,128]{2,1,0:T(8,128)(2,1)S(1)}, bf16[2048,384]{1,0:T(8,128)(2,1)S(1)}, bf16[2048,384]{1,0:T(8,128)(2,1)S(1)}, bf16[384,2048]{1,0:T(8,128)(2,1)S(1)}) custom-call(bf16[8,128,128]{2,1,0:T(8,128)(2,1)S(1)} %fusion.3.q_ref, bf16[8,2,128,128]{3,2,1,0:T(8,128)(2,1)S(1)} %pad_maximum_fusion.kv_ref, ...), custom_call_target="tpu_custom_call" | custom-call | tf_op jit(solution)/shard_map/pallas_call | solution.py:274
  165.4 1.1 copy-done
  166.6 1.2 copy-done.1
  167.7 1.2 copy-done.2
  168.9 0.7 copy-done.6
  169.6 54.3 %shard_map.137 = bf16[64,2048]{1,0:T(8,128)(2,1)} custom-call(bf16[8,128,128]{2,1,0:T(8,128)(2,1)} %copy-done.6, bf16[256,2048]{1,0:T(8,128)(2,1)} %on_ref.1, bf16[512,2048]{1,0:T(8,128)(2,1)} %ob_ref.1, bf16[128,2048]{1,0:T(8,128)(2,1)} %stream_ref.1, f32[1,2048]{1,0:T(1,128)} %bitcast.31, bf16[2048,384]{1,0:T(8,128)(2,1)} %copy-done, ...), custom_call_target="tpu_custom_call" | custom-call | tf_op jit(solution)/shard_map/pallas_call | solution.py:394
  223.9 1.7 copy.28
  (16 shorter events, 0.2 us)
Async XLA Ops:
  0.0 6.3 %copy-start.8 = (bf16[128,512]{1,0:T(8,128)(2,1)S(1)}, bf16[128,512]{1,0:T(8,128)(2,1)}, u32[]{:S(2)}) copy-start(bf16[128,512]{1,0:T(8,128)(2,1)} %param.20) | copy-start | bytes 393220
  0.0 6.0 %copy-start.7 = (bf16[128,512]{1,0:T(8,128)(2,1)S(1)}, bf16[128,512]{1,0:T(8,128)(2,1)}, u32[]{:S(2)}) copy-start(bf16[128,512]{1,0:T(8,128)(2,1)} %param.18) | copy-start | bytes 393220
  6.0 1.0 copy-start.3
  6.0 1.1 copy-start.4
  6.0 1.2 copy-start.5
  165.4 1.2 copy-start
  166.6 1.2 copy-start.1
  167.7 1.2 copy-start.2
  168.9 0.7 copy-start.6

commit v2 on v1

--- a/solution.py
+++ b/solution.py
@@ -78,26 +78,51 @@
         fcols = gate_all.shape[1]
         dcols = down_ref.shape[1]
 
-        def w_pieces(d, src):
-            part = pl.multiple_of((d % group) * fcols, 128)
-            at_rows = pl.ds(pl.multiple_of(src * drows, 128), drows)
-            at_cols = pl.ds(pl.multiple_of(src * dcols, 128), dcols)
-            return (
-                (gate_ref.at[:, pl.ds(part, fcols)], gate_all.at[at_rows, :], g_s, g_r),
-                (up_ref.at[:, pl.ds(part, fcols)], up_all.at[at_rows, :], u_s, u_r),
-                (down_ref.at[pl.ds(part, fcols), :], down_all.at[:, at_cols], d_s, d_r),
-            )
-
-        def w_copies(d, src, sem):
+        cols = n // group
+        mine, lane = me // cols, me % cols
+
+        def at_rows(src):
+            return pl.ds(pl.multiple_of(src * drows, 128), drows)
+
+        def at_cols(src):
+            return pl.ds(pl.multiple_of(src * dcols, 128), dcols)
+
+        def landing(src):
+            return (gate_all.at[at_rows(src), :], up_all.at[at_rows(src), :], down_all.at[:, at_cols(src)])
+
+        def raw(member):
+            part = pl.ds(pl.multiple_of(member * fcols, 128), fcols)
+            return (gate_ref.at[:, part], up_ref.at[:, part], down_ref.at[part, :])
+
+        def w_copies(sources, src, d, sem):
             return [
                 pltpu.make_async_remote_copy(
                     src_ref=a, dst_ref=b, send_sem=ss.at[sem], recv_sem=rs.at[src],
                     device_id={"sp": d}, device_id_type=MESH)
-                for a, b, ss, rs in w_pieces(d, src)
+                for a, b, ss, rs in zip(sources, landing(src), (g_s, u_s, d_s), (g_r, u_r, d_r))
             ]
 
         def w_local():
-            return [pltpu.make_async_copy(a, b, rs.at[me]) for a, b, ss, rs in w_pieces(me, me)]
+            return [
+                pltpu.make_async_copy(a, b, rs.at[me])
+                for a, b, rs in zip(raw(mine), landing(me), (g_r, u_r, d_r))
+            ]
+
+        def along(k):
+            return lax.rem(mine + k, group)
+
+        def beside(t):
+            return lax.rem(lane + t, cols)
+
+        def first_copies(k):
+            return w_copies(raw(along(k)), me, along(k) * cols + lane, k)
+
+        def own_copies(t):
+            return w_copies(raw(mine), me, mine * cols + beside(t), group + t)
+
+        def next_copies(k, t):
+            src = along(k) * cols + lane
+            return w_copies(landing(src), src, mine * cols + beside(t), group + k * cols + t)
 
     greet([(lambda t: {"sp": peer(t)}, n)])
 
@@ -120,19 +145,26 @@
         off_copy(d, me, t).start()
         return carry
 
+    if weights_too:
+        for k in range(1, group):
+            for c in first_copies(k):
+                c.start()
+        for t in range(1, cols):
+            for c in own_copies(t):
+                c.start()
     lax.fori_loop(1, n, send_kv, 0)
     lax.fori_loop(0, H, send_q, 0)
     pltpu.make_async_copy(kv_ref.at[head], kvbuf.at[me], kv_r.at[me]).start()
     pltpu.make_async_copy(off_ref.at[head], offbuf.at[me], off_r.at[me]).start()
     if weights_too:
-        def send_w(t, carry):
-            for c in w_copies(peer(t), me, t):
-                c.start()
-            return carry
-
-        lax.fori_loop(1, n, send_w, 0)
         for c in w_local():
             c.start()
+        for k in range(1, group):
+            src = along(k) * cols + lane
+            for index, c in enumerate(w_copies(landing(src), src, src, k)):
+                c.wait_recv()
+                for t in range(1, cols):
+                    next_copies(k, t)[index].start()
 
     row = lax.broadcasted_iota(jnp.int32, (WIDE, WIDE), 0)
     col = lax.broadcasted_iota(jnp.int32, (WIDE, WIDE), 1)
@@ -213,15 +245,23 @@
         d = peer(t)
         kv_copy(d, me, t).wait_send()
         off_copy(d, me, t).wait_send()
-        if weights_too:
-            for c in w_copies(d, me, t):
-                c.wait_send()
-            for c in w_copies(d, d, t):
-                c.wait_recv()
         return carry
 
     lax.fori_loop(1, n, wait_sends, 0)
     if weights_too:
+        for k in range(1, group):
+            for c in first_copies(k):
+                c.wait_send()
+        for t in range(1, cols):
+            for c in own_copies(t):
+                c.wait_send()
+            for k in range(group):
+                src = along(k) * cols + beside(t)
+                for c in w_copies(landing(src), src, src, 0):
+                    c.wait_recv()
+                if k:
+                    for c in next_copies(k, t):
+                        c.wait_send()
         for c in w_local():
             c.wait()
 
@@ -268,7 +308,7 @@
         cols = gate.shape[1] // group
         out_shape += [jax.ShapeDtypeStruct((gate.shape[0] * n, cols), jnp.bfloat16)] * 2
         out_shape += [jax.ShapeDtypeStruct((cols, down.shape[1] * n), jnp.bfloat16)]
-        scratch += [dma((n,))] * 6
+        scratch += [dma((group + n,)), dma((n,))] * 3
         args += [gate, up, down]
         specs += [hbm] * 3
     return pl.pallas_call(
@@ -283,22 +323,27 @@
     )(*args)
 
 
-def mix_kernel(a, T, hp, att_ref, on_ref, ob_ref, stream_ref, gain_ref, gate_ref, up_ref, down_ref,
-               out_ref, pbuf, prec, mid, xs, pb, ps, p_s, p_r, x_s, x_r, r_s, r_r):
-    G = a * T
+def mix_kernel(a, C, T, hp, att_ref, on_ref, ob_ref, stream_ref, gain_ref, gate_hbm, up_hbm, down_hbm,
+               out_ref, gate_ref, up_ref, down_ref, pbuf, prec, mid, xs, pb, pr, rsum, ps,
+               w_s, p_s, p_r, x_s, x_r, f_s, f_r, g_s, g_r, r_s, r_r):
     me = lax.axis_index("sp")
     j = lax.axis_index("tp")
-    base = (me // a) * a
-    g = (me - base) * T + j
+    z, c = me // C, me % C
     share = out_ref.shape[0]
-
-    def place(e):
-        return {"sp": base + e // T, "tp": e % T}
-
-    def other(t):
-        return lax.rem(g + t, G)
-
-    greet([(lambda t: place(other(t)), G)])
+    fetch = [
+        pltpu.make_async_copy(src, dst, w_s.at[i])
+        for i, (src, dst) in enumerate(((gate_hbm, gate_ref), (up_hbm, up_ref), (down_hbm, down_ref)))
+    ]
+    for copy in fetch:
+        copy.start()
+
+    def along(k):
+        return lax.rem(z + jnp.where(z < a // 2, k, a - k), a)
+
+    def core(t):
+        return lax.rem(j + t, T)
+
+    greet([(lambda t: {"sp": lax.rem(z + t, a) * C + c}, a), (lambda t: {"tp": core(t)}, T)])
 
     cut = [att_ref[h][:, :NARROW_SIZE] for h in range(hp)]
     part = jnp.dot(jnp.concatenate(cut, axis=1), on_ref[...], preferred_element_type=jnp.float32)
@@ -314,91 +359,121 @@
             device_id={"tp": to}, device_id_type=MESH)
 
     for t in range(1, T):
-        p_copy(lax.rem(j + t, T), j, t).start()
+        p_copy(core(t), j, t).start()
     total = pbuf[j].astype(jnp.float32)
     for t in range(1, T):
-        src = lax.rem(j + t, T)
+        src = core(t)
         p_copy(src, src, t).wait_recv()
         total = total + prec[src].astype(jnp.float32)
     own = pl.ds(pl.multiple_of(j * share, share), share)
     mid[...] = (stream_ref[own, :].astype(jnp.float32) + total).astype(jnp.bfloat16)
     middle = mid[...].astype(jnp.float32)
     scaled = middle * lax.rsqrt(jnp.mean(middle * middle, axis=1, keepdims=True) + norm_eps)
-    xs[g] = (scaled * gain_ref[...]).astype(jnp.bfloat16)
-
-    def x_copy(e, src, t):
-        return pltpu.make_async_remote_copy(
-            src_ref=xs.at[src], dst_ref=xs.at[src], send_sem=x_s.at[t], recv_sem=x_r.at[src],
-            device_id=place(e), device_id_type=MESH)
-
-    def r_copy(e, src):
-        return pltpu.make_async_remote_copy(
-            src_ref=pb.at[e], dst_ref=ps.at[src], send_sem=r_s.at[e], recv_sem=r_r.at[src],
-            device_id=place(e), device_id_type=MESH)
-
-    def send_x(t, carry):
-        x_copy(other(t), g, t).start()
-        return carry
-
-    lax.fori_loop(1, G, send_x, 0)
+    xs[z, j] = (scaled * gain_ref[...]).astype(jnp.bfloat16)
+
+    def x_copy(m, src, k):
+        return pltpu.make_async_remote_copy(
+            src_ref=xs.at[src, j], dst_ref=xs.at[src, j], send_sem=x_s.at[k], recv_sem=x_r.at[src],
+            device_id={"sp": m * C + c}, device_id_type=MESH)
+
+    def f_copy(m, to, src, t):
+        return pltpu.make_async_remote_copy(
+            src_ref=xs.at[m, src], dst_ref=xs.at[m, src], send_sem=f_s.at[m, t], recv_sem=f_r.at[m, src],
+            device_id={"tp": to}, device_id_type=MESH)
+
+    def g_copy(m, to, src, t):
+        return pltpu.make_async_remote_copy(
+            src_ref=pb.at[m, to], dst_ref=pr.at[m, src], send_sem=g_s.at[m, t], recv_sem=g_r.at[m, src],
+            device_id={"tp": to}, device_id_type=MESH)
+
+    def r_copy(m, src):
+        return pltpu.make_async_remote_copy(
+            src_ref=rsum.at[m], dst_ref=ps.at[src], send_sem=r_s.at[m], recv_sem=r_r.at[src],
+            device_id={"sp": m * C + c}, device_id_type=MESH)
+
+    for k in range(1, a):
+        x_copy(along(k), z, k).start()
+
+    def join(m):
+        total = pb[m, j].astype(jnp.float32)
+        for t in range(1, T):
+            g_copy(m, core(t), core(t), t).wait_recv()
+            total = total + pr[m, core(t)].astype(jnp.float32)
+        rsum[m] = total.astype(jnp.bfloat16)
 
     def one_member(k, carry):
-        m = lax.rem(me - base + k, a)
-        for s in range(T):
-            e = m * T + s
-
-            @pl.when(e != g)
-            def _():
-                x_copy(e, e, 0).wait_recv()
-
-        x = xs[pl.ds(m * T, T)].reshape(T * share, xs.shape[2])
+        m = along(k)
+
+        @pl.when(k > 0)
+        def _():
+            x_copy(m, m, 0).wait_recv()
+
+        for t in range(1, T):
+            f_copy(m, core(t), j, t).start()
+
+        @pl.when(k == 0)
+        def _():
+            for copy in fetch:
+                copy.wait()
+
+        @pl.when(k > 1)
+        def _():
+            join(along(k - 1))
+            r_copy(along(k - 1), z).start()
+
+        for t in range(1, T):
+            f_copy(m, core(t), core(t), t).wait_recv()
+        x = xs[m].reshape(T * share, xs.shape[3])
         gate = jnp.dot(x, gate_ref[...], preferred_element_type=jnp.float32)
         up = jnp.dot(x, up_ref[...], preferred_element_type=jnp.float32)
         hidden = (gate / (1.0 + jnp.exp(-gate)) * up).astype(jnp.bfloat16)
         mixed = jnp.dot(hidden, down_ref[...], preferred_element_type=jnp.float32)
-        pb[pl.ds(m * T, T)] = mixed.astype(jnp.bfloat16).reshape(T, share, mixed.shape[1])
-        for s in range(T):
-            e = m * T + s
-
-            @pl.when(e != g)
-            def _():
-                r_copy(e, g).start()
-
+        pb[m] = mixed.astype(jnp.bfloat16).reshape(T, share, mixed.shape[1])
+        for t in range(1, T):
+            g_copy(m, core(t), j, t).start()
         return carry
 
     lax.fori_loop(0, a, one_member, 0)
-    total = pb[g].astype(jnp.float32)
-    for t in range(1, G):
-        e = other(t)
-        r_copy(e, e).wait_recv()
-        total = total + ps[e].astype(jnp.float32)
+    if a > 1:
+        join(along(a - 1))
+        r_copy(along(a - 1), z).start()
+    join(z)
+    total = rsum[z].astype(jnp.float32)
+    for k in range(1, a):
+        m = along(k)
+        r_copy(m, m).wait_recv()
+        total = total + ps[m].astype(jnp.float32)
     out_ref[...] = (mid[...].astype(jnp.float32) + total).astype(jnp.bfloat16)
     for t in range(1, T):
-        p_copy(lax.rem(j + t, T), j, t).wait_send()
-
-    def finish(t, carry):
-        x_copy(other(t), g, t).wait_send()
-        r_copy(other(t), g).wait_send()
-        return carry
-
-    lax.fori_loop(1, G, finish, 0)
-
-
-def mix(a, T, hp, att, out_narrow, out_broad, stream, gain, gate, up, down):
-    G = a * T
+        p_copy(core(t), j, t).wait_send()
+        for m in range(a):
+            f_copy(m, core(t), j, t).wait_send()
+            g_copy(m, core(t), j, t).wait_send()
+    for k in range(1, a):
+        x_copy(along(k), z, k).wait_send()
+        r_copy(along(k), z).wait_send()
+
+
+def mix(n, a, T, hp, att, out_narrow, out_broad, stream, gain, gate, up, down):
     rows, width = stream.shape
     share = rows // T
     dma = pltpu.SemaphoreType.DMA
-    block = pltpu.VMEM((G, share, width), jnp.bfloat16)
+    block = pltpu.VMEM((a, T, share, width), jnp.bfloat16)
+    line = pltpu.VMEM((a, share, width), jnp.bfloat16)
     pair = pltpu.VMEM((T, share, width), jnp.bfloat16)
+    vmem = pl.BlockSpec(memory_space=pltpu.VMEM)
+    hbm = pl.BlockSpec(memory_space=pl.ANY)
     return pl.pallas_call(
-        functools.partial(mix_kernel, a, T, hp),
+        functools.partial(mix_kernel, a, n // a, T, hp),
         out_shape=jax.ShapeDtypeStruct((share, width), jnp.bfloat16),
-        in_specs=[pl.BlockSpec(memory_space=pltpu.VMEM)] * 8,
-        out_specs=pl.BlockSpec(memory_space=pltpu.VMEM),
+        in_specs=[vmem] * 5 + [hbm] * 3,
+        out_specs=vmem,
         scratch_shapes=[
-            pair, pair, pltpu.VMEM((share, width), jnp.bfloat16), block, block, block,
-            dma((T,)), dma((T,)), dma((G,)), dma((G,)), dma((G,)), dma((G,)),
+            pltpu.VMEM(gate.shape, gate.dtype), pltpu.VMEM(up.shape, up.dtype),
+            pltpu.VMEM(down.shape, down.dtype),
+            pair, pair, pltpu.VMEM((share, width), jnp.bfloat16), block, block, block, line, line,
+            dma((3,)), dma((T,)), dma((T,)), dma((a,)), dma((a,)), dma((a, T)), dma((a, T)),
+            dma((a, T)), dma((a, T)), dma((a,)), dma((a,)),
         ],
         compiler_params=pltpu.CompilerParams(
             collective_id=1, has_side_effects=True, vmem_limit_bytes=60 * 1024 * 1024
@@ -449,7 +524,7 @@
             n, hp, rows, group, q, kv, off, (gate_weight, up_weight, down_weight)
         )
         return mix(
-            group, T, hp, att, out_narrow, out_broad, stream, norm_gain, gate_all, up_all, down_all
+            n, group, T, hp, att, out_narrow, out_broad, stream, norm_gain, gate_all, up_all, down_all
         )
     att = attend(n, hp, rows, 0, q, kv, off, None)[0]
     attended_narrow = jnp.transpose(att[:hp, :, :NARROW_SIZE], (1, 0, 2)).reshape(rows, -1)

time: 227 us -> 158 us (0.70)
  Pallas kernels: 212 us -> 143 us
    pallas_call x1, Pallas kernels: 158 us -> 79.2 us  [attend(): pl.pallas_call(functools.partial(attend_kernel, n, hp, rows, group), out_...]
    pallas_call x1, Pallas kernels: 54.3 us -> 64 us  [mix(): pl.pallas_call(functools.partial(mix_kernel, a, n // a, T, hp), out_shape...]
where the time goes in v2:
time: 158 us; the launch traced here: 156 us
  Pallas kernels  143 us (91%)
  local copies, waits for them, and re-layouts  12.8 us (8%)
    pallas_call x1, Pallas kernels, attend(): pl.pallas_call(functools.partial(attend_kernel, n, hp, rows, group), out_...  79.2 us
    pallas_call x1, Pallas kernels, mix(): pl.pallas_call(functools.partial(mix_kernel, a, n // a, T, hp), out_shape...  64 us
    unnamed x25, local copies, waits for them, and re-layouts  10.5 us

profile of v2, /device:TPU:0, one launch (start us, length us, event | category | flops | bytes accessed | tf_op | source)
XLA Modules:
  0.0 156.3 jit_solution(9679854330764839851)
XLA Ops:
  0.0 0.7 slice.7
  0.7 0.7 slice.6
  1.5 0.9 copy.15
  2.4 0.1 copy.16
  2.6 1.0 copy.19
  3.5 0.1 copy.20
  3.7 1.0 copy.23
  4.6 0.1 copy.24
  4.8 1.0 copy.17
  5.8 0.1 copy.18
  6.0 0.1 copy.21
  6.1 0.1 copy.22
  6.3 0.1 copy.25
  6.4 0.1 copy.26
  6.7 0.3 copy-done.3
  7.0 0.1 copy-done.4
  7.1 0.1 copy-done.5
  7.2 79.2 %shard_map.136 = (bf16[8,128,128]{2,1,0:T(8,128)(2,1)S(1)}, bf16[2048,384]{1,0:T(8,128)(2,1)S(1)}, bf16[2048,384]{1,0:T(8,128)(2,1)S(1)}, bf16[384,2048]{1,0:T(8,128)(2,1)S(1)}) custom-call(bf16[8,128,128]{2,1,0:T(8,128)(2,1)S(1)} %fusion.3.q_ref, bf16[8,2,128,128]{3,2,1,0:T(8,128)(2,1)S(1)} %pad_maximum_fusion.kv_ref, ...), custom_call_target="tpu_custom_call" | custom-call | tf_op jit(solution)/shard_map/pallas_call | solution.py:314
  86.4 1.1 copy-done
  87.6 1.2 copy-done.1
  88.7 1.2 copy-done.2
  89.9 0.7 copy-done.6
  90.6 64.0 %shard_map.137 = bf16[64,2048]{1,0:T(8,128)(2,1)} custom-call(bf16[8,128,128]{2,1,0:T(8,128)(2,1)} %copy-done.6, bf16[256,2048]{1,0:T(8,128)(2,1)} %on_ref.1, bf16[512,2048]{1,0:T(8,128)(2,1)} %ob_ref.1, bf16[128,2048]{1,0:T(8,128)(2,1)} %stream_ref.1, f32[1,2048]{1,0:T(1,128)} %bitcast.31, bf16[2048,384]{1,0:T(8,128)(2,1)} %copy-done, ...), custom_call_target="tpu_custom_call" | custom-call | tf_op jit(solution)/shard_map/pallas_call | solution.py:466
  154.6 1.7 %copy.28 = bf16[64,2048]{1,0:T(8,128)(2,1)} copy(bf16[64,2048]{1,0:T(8,128)(2,1)} %shard_map.137) | data formatting | bytes 524288
  (16 shorter events, 0.2 us)
Async XLA Ops:
  0.0 6.3 %copy-start.8 = (bf16[128,512]{1,0:T(8,128)(2,1)S(1)}, bf16[128,512]{1,0:T(8,128)(2,1)}, u32[]{:S(2)}) copy-start(bf16[128,512]{1,0:T(8,128)(2,1)} %param.20) | copy-start | bytes 393220
  0.0 6.0 %copy-start.7 = (bf16[128,512]{1,0:T(8,128)(2,1)S(1)}, bf16[128,512]{1,0:T(8,128)(2,1)}, u32[]{:S(2)}) copy-start(bf16[128,512]{1,0:T(8,128)(2,1)} %param.18) | copy-start | bytes 393220
  6.0 1.0 copy-start.3
  6.0 1.1 copy-start.4
  6.0 1.2 copy-start.5
  86.4 1.2 copy-start
  87.6 1.2 copy-start.1
  88.7 1.2 copy-start.2
  89.9 0.7 copy-start.6
